TPU v7x, 32 devices: a whole 2x2x4 slice. The times are simulated.
32 devices in a mesh: ra: 4 (over z), cb: 4 (over y, x), dp: 2 (over core).
Axes of the slice: x: 2, y: 2, z: 4, core: 2. Of those that a mesh axis runs over, the one named last changes fastest.
Arguments:
- tokens: bfloat16 [3072, 4096], P('dp', 'ra'), may hold values from -20 to 20
- pre_gain: float32 [4096], P('ra'), may hold values from 0.1 to 1.9
- up_weight: bfloat16 [4096, 16384], P('ra', 'cb'), may hold values from -0.09375 to 0.09375
- up_bias: float32 [16384], P('cb'), may hold values from -4 to 4
- down_weight: bfloat16 [16384, 4096], P('cb', 'ra'), may hold values from -0.046875 to 0.046875
- post_gain: float32 [4096], P('ra'), may hold values from 0.1 to 1.9
Outputs:
- stream_out: bfloat16 [3072, 4096], P('dp', 'ra')
All inputs are finite; a program needn't handle non-finite values.
Results may differ from a plain program's by a relative error of at most 0.0051.
Values may be sent and summed in bfloat16 or wider, within the bound.
A program may use at most 128 MiB of HBM per device.

v0:
```python
import jax
import jax.numpy as jnp
from jax import lax
from jax.sharding import PartitionSpec as P

D = 4096
epsilon = 1e-06
residual_weight = 0.5


def activate(summed, inverse, offset):
    return jnp.square(jax.nn.relu(summed * inverse[:, None] + offset)).astype(jnp.bfloat16)


def body(tokens, pre_gain, up_weight, up_bias, down_weight, post_gain):
    stream = tokens.astype(jnp.float32)
    energy = jnp.sum(stream * stream, axis=1)
    scaled = (stream * pre_gain).astype(jnp.bfloat16)
    partial_value = jnp.dot(scaled, up_weight, preferred_element_type=jnp.float32)
    total = lax.psum(energy, "ra")
    share = lax.psum_scatter(partial_value, "ra", scatter_dimension=1, tiled=True)
    width = share.shape[1]
    offset = lax.dynamic_slice_in_dim(up_bias, lax.axis_index("ra") * width, width, 0)
    hidden = activate(share, lax.rsqrt(total / D + epsilon), offset)
    branch = jnp.dot(
        lax.all_gather(hidden, "ra", axis=1, tiled=True),
        down_weight,
        preferred_element_type=jnp.float32,
    )
    branch = lax.psum(branch, "cb")
    branch_energy = lax.psum(jnp.sum(branch * branch, axis=1), "ra")
    normed = branch * lax.rsqrt(branch_energy / D + epsilon)[:, None] * post_gain
    return (residual_weight * stream + normed).astype(jnp.bfloat16)


def solution(mesh):
    in_specs = (P("dp", "ra"), P("ra"), P("ra", "cb"), P("cb"), P("cb", "ra"), P("ra"))
    out_specs = P("dp", "ra")
    return jax.shard_map(body, mesh=mesh, in_specs=in_specs, out_specs=out_specs, check_vma=False)
```

profile of v0, /device:TPU:0, one launch (start us, length us, event | category | flops | bytes accessed | tf_op | source)
XLA Modules:
  0.0 853.5 jit_solution(10800701514293128842)
XLA Ops:
  6.5 0.0 reduce-scatter.2.cloned.1.call-start
  6.5 21.1 %fusion.4 = f32[1536,4096]{1,0:T(8,128)} fusion(bf16[1024,4096]{1,0:T(8,128)(2,1)} %param.8, bf16[1536,1024]{1,0:T(8,128)(2,1)} %param.6, f32[1024]{0:T(1024)} %param.7), kind=kOutput, calls=%fused_computation.9 | convolution fusion | flops 12889620480 | bytes 36704256 | tf_op jit(solution)/shard_map/dot_general | solution.py:19
  27.7 0.0 copy-start
  27.7 0.0 reduce-scatter.2.cloned.1.call-update
  27.7 0.0 all-gather.2.cloned.1.call-start
  27.8 0.8 dynamic_slice.3
  28.6 1.0 copy-done
  29.6 0.7 fusion.3
  30.3 14.3 %psum.21 = f32[1536]{0:T(1024)S(1)} all-reduce(f32[1536]{0:T(1024)S(1)} %fusion.3), channel_id=1, replica_groups=mesh['ra'=4,'cb'=4,'dp'=2] {'ra'}, use_global_device_ids=true, to_apply=%region_2.0 | all-reduce | flops 1536 | bytes 12288 | tf_op jit(solution)/shard_map/psum | solution.py:20
  44.6 400.5 %reduce-scatter.2.cloned.1.call-done = f32[1536,1024]{1,0:T(8,128)} async-done(((f32[1536,4096]{1,0:T(8,128)}), f32[1536,1024]{1,0:T(8,128)}) %reduce-scatter.2.cloned.1.call-update) | async-done | bytes 6291472 | tf_op jit(solution)/shard_map/reduce_scatter | solution.py:21
  445.2 5.4 multiply_convert_fusion
  450.6 0.0 all-gather.2.cloned.1.call-update
  450.6 0.0 all-reduce.2.cloned.1.call-start
  450.7 220.3 %all-gather.2.cloned.1.call-done = bf16[1536,4096]{1,0:T(8,128)(2,1)} async-done(((bf16[1536,1024]{1,0:T(8,128)(2,1)}), bf16[1536,4096]{1,0:T(8,128)(2,1)}) %all-gather.2.cloned.1.call-update) | async-done | bytes 12582928 | tf_op jit(solution)/shard_map/all_gather | solution.py:26
  671.0 19.5 %fusion.7 = f32[1536,1024]{1,0:T(8,128)} fusion(bf16[1536,4096]{1,0:T(8,128)(2,1)} %all-gather.2.cloned.1.call-done, bf16[4096,1024]{1,0:T(8,128)(2,1)} %param.10), kind=kOutput, calls=%fused_computation.13 | convolution fusion | flops 12884901888 | bytes 27262976 | tf_op jit(solution)/shard_map/dot_general | solution.py:25
  690.5 0.0 copy-start.1
  690.5 0.0 all-reduce.2.cloned.1.call-update
  690.5 136.5 %all-reduce.2.cloned.1.call-done = f32[1536,1024]{1,0:T(8,128)} async-done(((f32[1536,1024]{1,0:T(8,128)}), f32[1536,1024]{1,0:T(8,128)}) %all-reduce.2.cloned.1.call-update) | async-done | bytes 6291472 | tf_op jit(solution)/shard_map/psum | solution.py:30
  827.0 3.3 multiply_reduce_fusion
  830.3 11.9 %psum.23 = f32[1536]{0:T(1024)S(1)} all-reduce(f32[1536]{0:T(1024)S(1)} %multiply_reduce_fusion), channel_id=1, replica_groups=mesh['ra'=4,'cb'=4,'dp'=2] {'ra'}, use_global_device_ids=true, to_apply=%region_5.6 | all-reduce | flops 1536 | bytes 12288 | tf_op jit(solution)/shard_map/psum | solution.py:31
  842.3 0.0 copy-done.1
  842.3 4.7 fusion.1
  (2 shorter events, 0.0 us)
Async XLA Ops:
  6.5 438.6 %reduce-scatter.2.cloned.1.call-start = ((), (), s32[]{:S(2)}) async-start(), calls=%async_computation.1 | async-start | bytes 31457280 | tf_op jit(solution)/shard_map/reduce_scatter | solution.py:21
  27.7 1.9 copy-start
  27.7 643.3 %all-gather.2.cloned.1.call-start = ((), (), s32[]{:S(2)}) async-start(), calls=%async_computation.2 | async-start | bytes 15728640 | tf_op jit(solution)/shard_map/all_gather | solution.py:26
  450.6 376.4 %all-reduce.2.cloned.1.call-start = ((), (), s32[]{:S(2)}) async-start(), calls=%async_computation.3 | async-start | bytes 12582912 | tf_op jit(solution)/shard_map/psum | solution.py:30
  690.5 151.8 %copy-start.1 = (f32[1024]{0:T(1024)S(1)}, f32[1024]{0:T(1024)}, u32[]{:S(2)}) copy-start(f32[1024]{0:T(1024)} %param.11) | copy-start | bytes 12292
Sparse Core Ops, SparseCore 0:
  27.8 417.2 reduce-scatter.1
  450.7 220.2 all-gather.1
  690.6 136.3 all-reduce.1
where the time goes:
time: 854 us
  waiting for transfers between devices  757 us (89%)
  matrix products  40.6 us (5%)
  blocking collectives  26.3 us (3%)
  other arithmetic  14.1 us (2%)
  between operations  13.2 us (2%)
    reduce_scatter x1, waiting for transfers between devices, body(): lax.psum_scatter(partial_value, 'ra', scatter_dimension=1, tiled=True)  401 us
    all_gather x1, waiting for transfers between devices, body(): lax.all_gather(hidden, 'ra', axis=1, tiled=True)  220 us
    psum x1, waiting for transfers between devices, body(): branch = lax.psum(branch, 'cb')  137 us
    dot_general x1, matrix products, body(): jnp.dot(scaled, up_weight, preferred_element_type=jnp.float32)  21.1 us
    dot_general x1, matrix products, body(): jnp.dot(lax.all_gather(hidden, 'ra', axis=1, tiled=True), down_weight, pr...  19.5 us
  transfers between devices with their start and end apart: 3, of which 3 were waited for; matrix products, arithmetic and copies ran while one was open for 0% of the time, Pallas kernels for 0%

commit v1 on v0

--- a/solution.py
+++ b/solution.py
@@ -27,7 +27,11 @@
         down_weight,
         preferred_element_type=jnp.float32,
     )
-    branch = lax.psum(branch, "cb")
+    size, acc = (lax.axis_size("cb"), branch)
+    for reach in [1 << k for k in range(size.bit_length() - 1)]:
+        swap = [(i, i ^ reach) for i in range(size)]
+        acc = acc + lax.ppermute(acc, "cb", swap)
+    branch = acc
     branch_energy = lax.psum(jnp.sum(branch * branch, axis=1), "ra")
     normed = branch * lax.rsqrt(branch_energy / D + epsilon)[:, None] * post_gain
     return (residual_weight * stream + normed).astype(jnp.bfloat16)

time: 854 us -> 1000 us (1.17)
  waiting for transfers between devices: 757 us -> 893 us
    ppermute x0 -> x2, waiting for transfers between devices: none -> 271 us  [body(): acc = acc + lax.ppermute(acc, 'cb', swap)]
    psum x1 -> x0, waiting for transfers between devices: 137 us -> none  [body(): branch = lax.psum(branch, 'cb')]
  transfers between devices with their start and end apart: 3 -> 4, of which waited for: 3 -> 4; matrix products, arithmetic and copies ran while one was open for 0% -> 0% of each run, Pallas kernels for 0% -> 0%
where the time goes in v1:
time: 1000 us
  waiting for transfers between devices  893 us (89%)
  matrix products  38.4 us (4%)
  blocking collectives  23.2 us (2%)
  other arithmetic  20 us (2%)
  between operations  13.5 us (1%)
    reduce_scatter x1, waiting for transfers between devices, body(): lax.psum_scatter(partial_value, 'ra', scatter_dimension=1, tiled=True)  401 us
    ppermute x2, waiting for transfers between devices, body(): acc = acc + lax.ppermute(acc, 'cb', swap)  271 us
    all_gather x1, waiting for transfers between devices, body(): lax.all_gather(hidden, 'ra', axis=1, tiled=True)  220 us
    dot_general x1, matrix products, body(): jnp.dot(scaled, up_weight, preferred_element_type=jnp.float32)  20.5 us
  transfers between devices with their start and end apart: 4, of which 4 were waited for; matrix products, arithmetic and copies ran while one was open for 0% of the time, Pallas kernels for 0%

profile of v1, /device:TPU:0, one launch (start us, length us, event | category | flops | bytes accessed | tf_op | source)
XLA Modules:
  0.0 999.7 jit_solution(1805430019566300692)
XLA Ops:
  6.5 0.0 copy-start.1
  6.5 0.0 reduce-scatter.2.cloned.1.call-start
  6.5 3.2 copy.7
  9.7 0.0 copy-done.1
  9.7 20.5 %fusion.4 = f32[1536,4096]{1,0:T(8,128)} fusion(bf16[1024,4096]{1,0:T(8,128)(2,1)} %param.8, bf16[1536,1024]{0,1:T(8,128)(2,1)S(1)} %copy.7, f32[1024]{0:T(1024)S(1)} %copy-done.1), kind=kOutput, calls=%fused_computation.9 | convolution fusion | flops 12889620480 | bytes 36704256 | tf_op jit(solution)/shard_map/dot_general | solution.py:19
  30.2 0.0 reduce-scatter.2.cloned.1.call-update
  30.2 0.0 all-gather.2.cloned.1.call-start
  30.3 0.7 dynamic_slice.3
  31.0 0.7 fusion.3
  31.6 14.4 %psum.14 = f32[1536]{0:T(1024)S(1)} all-reduce(f32[1536]{0:T(1024)S(1)} %fusion.3), channel_id=1, replica_groups=mesh['ra'=4,'cb'=4,'dp'=2] {'ra'}, use_global_device_ids=true, to_apply=%region_2.0 | all-reduce | flops 1536 | bytes 12288 | tf_op jit(solution)/shard_map/psum | solution.py:20
  46.1 401.4 %reduce-scatter.2.cloned.1.call-done = f32[1536,1024]{1,0:T(8,128)} async-done(((f32[1536,4096]{1,0:T(8,128)}), f32[1536,1024]{1,0:T(8,128)}) %reduce-scatter.2.cloned.1.call-update) | async-done | bytes 6291472 | tf_op jit(solution)/shard_map/reduce_scatter | solution.py:21
  447.5 5.4 multiply_convert_fusion
  452.9 0.0 all-gather.2.cloned.1.call-update
  452.9 220.4 %all-gather.2.cloned.1.call-done = bf16[1536,4096]{1,0:T(8,128)(2,1)} async-done(((bf16[1536,1024]{1,0:T(8,128)(2,1)}), bf16[1536,4096]{1,0:T(8,128)(2,1)}) %all-gather.2.cloned.1.call-update) | async-done | bytes 12582928 | tf_op jit(solution)/shard_map/all_gather | solution.py:26
  673.4 17.9 %fusion.7 = f32[1536,1024]{0,1:T(8,128)S(1)} fusion(bf16[1536,4096]{1,0:T(8,128)(2,1)} %all-gather.2.cloned.1.call-done, bf16[4096,1024]{1,0:T(8,128)(2,1)} %param.10), kind=kOutput, calls=%fused_computation.13 | convolution fusion | flops 12884901888 | bytes 27262976 | tf_op jit(solution)/shard_map/dot_general | solution.py:25
  691.3 1.5 collective-permute-start
  692.8 136.1 %collective-permute-done = f32[1536,1024]{0,1:T(8,128)} collective-permute-done((f32[1536,1024]{0,1:T(8,128)S(1)}, f32[1536,1024]{0,1:T(8,128)}, u32[]{:S(2)}, u32[]{:S(2)}) %collective-permute-start) | collective-permute-done | bytes 6291488 | tf_op jit(solution)/shard_map/ppermute | solution.py:33
  828.9 4.2 add.36
  833.1 0.0 copy-start
  833.1 1.5 collective-permute-start.1
  834.6 135.1 %collective-permute-done.1 = f32[1536,1024]{0,1:T(8,128)S(1)} collective-permute-done((f32[1536,1024]{0,1:T(8,128)S(1)}, f32[1536,1024]{0,1:T(8,128)S(1)}, u32[]{:S(2)}, u32[]{:S(2)}) %collective-permute-start.1) | collective-permute-done | bytes 6291488 | tf_op jit(solution)/shard_map/ppermute | solution.py:33
  969.7 4.1 multiply_reduce_fusion
  973.8 8.8 psum.15
  982.6 0.0 copy-done
  982.6 5.7 fusion.1
  988.2 4.6 copy.8
  (2 shorter events, 0.0 us)
Async XLA Ops:
  6.5 3.2 copy-start.1
  6.5 440.9 %reduce-scatter.2.cloned.1.call-start = ((), (), s32[]{:S(2)}) async-start(), calls=%async_computation.1 | async-start | bytes 31457280 | tf_op jit(solution)/shard_map/reduce_scatter | solution.py:21
  30.2 643.1 %all-gather.2.cloned.1.call-start = ((), (), s32[]{:S(2)}) async-start(), calls=%async_computation.2 | async-start | bytes 15728640 | tf_op jit(solution)/shard_map/all_gather | solution.py:26
  691.3 137.6 %collective-permute-start = (f32[1536,1024]{0,1:T(8,128)S(1)}, f32[1536,1024]{0,1:T(8,128)}, u32[]{:S(2)}, u32[]{:S(2)}) collective-permute-start(f32[1536,1024]{0,1:T(8,128)S(1)} %fusion.7), channel_id=1, source_target_pairs={{0,2},{2,0},{4,6},{6,4},{1,3},{3,1},{5,7},{7,5},{8,10},{10,8},{12,... | collective-permute-start | bytes 18874376 | tf_op jit(solution)/shard_map/ppermute | solution.py:33
  833.1 149.5 %copy-start = (f32[1024]{0:T(1024)S(1)}, f32[1024]{0:T(1024)}, u32[]{:S(2)}) copy-start(f32[1024]{0:T(1024)} %param.11) | copy-start | bytes 12292
  833.1 136.6 %collective-permute-start.1 = (f32[1536,1024]{0,1:T(8,128)S(1)}, f32[1536,1024]{0,1:T(8,128)S(1)}, u32[]{:S(2)}, u32[]{:S(2)}) collective-permute-start(f32[1536,1024]{0,1:T(8,128)S(1)} %add.36), channel_id=1, source_target_pairs={{0,4},{2,6},{4,0},{6,2},{1,5},{3,7},{5,1},{7,3},{8,12},{10,14},{12... | collective-permute-start | bytes 18874376 | tf_op jit(solution)/shard_map/ppermute | solution.py:33
Sparse Core Ops, SparseCore 0:
  30.3 417.0 reduce-scatter.1
  453.1 220.2 all-gather.1
